TPU v7x, 32 devices: a whole 2x2x4 slice. The times are simulated.
32 devices in a mesh: tp: 8 (over z, y), dp: 4 (over x, core).
Axes of the slice: x: 2, y: 2, z: 4, core: 2. Of those that a mesh axis runs over, the one named last changes fastest.
Arguments:
- stream: bfloat16 [256, 2048], P('tp', 'dp'), may hold values from -12 to 12
- norm_gain: float32 [2, 2048], P(None, 'dp'), may hold values from 0.1 to 1.9
- w_input: bfloat16 [2, 2048, 2048], P(None, 'dp', 'tp'), may hold values from -0.125 to 0.125
- lam_re: float32 [2, 128, 64], P(None, 'tp'), may hold values from -1 to -0.05
- lam_im: float32 [2, 128, 64], P(None, 'tp'), may hold values from 0 to 6
- log_dt: float32 [2, 128], P(None, 'tp'), may hold values from -3 to 0
- b_re: float32 [2, 128, 64, 16], P(None, 'tp'), may hold values from -1 to 1
- b_im: float32 [2, 128, 64, 16], P(None, 'tp'), may hold values from -1 to 1
- readout_real: float32 [2, 128, 16, 64], P(None, 'tp'), may hold values from -0.5 to 0.5
- readout_imaginary: float32 [2, 128, 16, 64], P(None, 'tp'), may hold values from -0.5 to 0.5
- d_skip: float32 [2, 2048], P(None, 'tp'), may hold values from -4 to 4
- w_val: bfloat16 [2, 2048, 2048], P(None, 'tp', 'dp'), may hold values from -0.375 to 0.375
- w_gate: bfloat16 [2, 2048, 2048], P(None, 'tp', 'dp'), may hold values from -0.375 to 0.375
- state: float32 [2, 256, 128, 128], P(None, 'dp', 'tp'), may hold values from -6 to 6
Outputs:
- stream_out: bfloat16 [256, 2048], P('tp', 'dp')
- states_out: float32 [2, 256, 128, 128], P(None, 'dp', 'tp')
All inputs are finite; a program needn't handle non-finite values.
Results may differ from a plain program's by a relative error of at most 0.0064.
Values may be sent and summed in bfloat16 or wider, within the bound.
A program may use at most 64 MiB of HBM per device.

v0:
```python
import functools

import jax
import jax.numpy as jnp
from jax import lax
from jax.experimental import pallas as pl
from jax.experimental.pallas import tpu as pltpu
from jax.sharding import PartitionSpec as P

EPS = 1e-06
F32 = jnp.float32
BF16 = jnp.bfloat16
HIGHEST = lax.Precision.HIGHEST
NT = (((1,), (1,)), ((), ()))


def partner(me, k, n, back=False):
    if n & (n - 1):
        return (me + (n - k if back else k)) % n
    found, bit = 0, 1
    while bit < n:
        mine = (me // bit) % 2
        found = found + (bit * (1 - mine) if k & bit else bit * mine)
        bit *= 2
    return found


def kernel(
    tp, dp, chans,
    stream_ref, gain_ref, w_in_hbm, lam_re_ref, lam_im_ref, log_dt_ref, b_re_hbm, b_im_hbm, c_re_hbm, c_im_hbm, skip_ref,
    w_val_hbm, w_gate_hbm, state_hbm,
    out_ref, state,
    w_in, w_val, w_gate, b_re, b_im, c_re, c_im, drive, read,
    kept, proj, u_keep, masked, from_old, mix_w,
    x_all, part_send, part_recv, sq_send, sq_recv, mix_all, block, comb_send, comb_own, pair_recv, comb_recv,
    load_sem, x_ss, x_rs, part_ss, part_rs, sq_ss, sq_rs, mix_ss, mix_rs, pair_ss, pair_rs, comb_ss, comb_rs,
):
    layers = w_in.shape[0]
    me_t, me_d = lax.axis_index("tp"), lax.axis_index("dp")
    rows_t, feats = stream_ref.shape
    rows_d, width = u_keep.shape[1:]
    per = rows_d // rows_t
    me_p, side = me_t // 2, me_t % 2
    groups, half = lam_re_ref.shape[1:]
    lanes = state.shape[2]
    sq_width = sq_send.shape[3]

    loads = {}
    for l in range(layers):
        for i, (src, dst) in enumerate(
            (
                (b_re_hbm, b_re), (b_im_hbm, b_im), (c_re_hbm, c_re), (c_im_hbm, c_im), (state_hbm, state),
                (w_in_hbm, w_in), (w_val_hbm, w_val), (w_gate_hbm, w_gate),
            )
        ):
            loads[l, i] = pltpu.make_async_copy(src.at[l], dst.at[l], load_sem.at[l, i])
            loads[l, i].start()

    barrier = pltpu.get_barrier_semaphore()
    for k in range(1, dp):
        pl.semaphore_signal(barrier, inc=1, device_id={"dp": partner(me_d, k, dp)}, device_id_type=pl.DeviceIdType.MESH)
    for k in range(1, tp):
        pl.semaphore_signal(barrier, inc=1, device_id={"tp": partner(me_t, k, tp)}, device_id_type=pl.DeviceIdType.MESH)

    def send(src, dst, ss, rs, axis, to):
        return pltpu.make_async_remote_copy(
            src_ref=src, dst_ref=dst, send_sem=ss, recv_sem=rs, device_id={axis: to}, device_id_type=pl.DeviceIdType.MESH
        )

    def x_copy(l, k):
        src = stream_ref if l == 0 else x_all.at[l, me_t]
        to = partner(me_t, k, tp)
        return send(src, x_all.at[l, me_t], x_ss.at[l, to], x_rs.at[l, me_t], "tp", to)

    def part_copy(l, to):
        return send(part_send.at[l, to], part_recv.at[l, me_d], part_ss.at[l, to], part_rs.at[l, me_d], "dp", to)

    def sq_copy(l, to):
        return send(sq_send.at[l, to], sq_recv.at[l, me_d], sq_ss.at[l, to], sq_rs.at[l, me_d], "dp", to)

    def mix_copy(l, to):
        return send(mix_all.at[l, me_d], mix_all.at[l, me_d], mix_ss.at[l, to], mix_rs.at[l, me_d], "dp", to)

    def comb_copy(l, to):
        return send(
            comb_send.at[l, 2 * to + side], comb_recv.at[l, me_p], comb_ss.at[l, to], comb_rs.at[l, me_p], "tp", 2 * to + side
        )

    def pair_copy(l, q):
        return send(
            comb_send.at[l, 2 * q + 1 - side], pair_recv.at[l, q], pair_ss.at[l, q], pair_rs.at[l, q], "tp", 2 * me_p + 1 - side
        )

    def arrival(ref, rs, axis):
        return send(ref, ref, rs, rs, axis, 0)

    lane_group = lax.broadcasted_iota(jnp.int32, (rows_d, width), 1) // chans
    eye = lax.broadcasted_iota(jnp.int32, (rows_d, sq_width), 0) == lax.broadcasted_iota(jnp.int32, (rows_d, sq_width), 1)

    group_eye = lax.broadcasted_iota(jnp.int32, (groups, groups), 0) == lax.broadcasted_iota(jnp.int32, (groups, groups), 1)

    def prepare(l):
        step_size = jnp.exp(jnp.sum(jnp.where(group_eye, log_dt_ref[l : l + 1, :], 0.0), axis=1, keepdims=True))
        lam_re, lam_im = lam_re_ref[l], lam_im_ref[l]
        decay = jnp.exp(lam_re * step_size)
        angle = lam_im * step_size
        keep_re = decay * jnp.cos(angle)
        keep_im = decay * jnp.sin(angle)
        denom = lam_re * lam_re + lam_im * lam_im
        ratio_re = ((keep_re - 1.0) * lam_re + keep_im * lam_im) / denom
        ratio_im = (keep_im * lam_re - (keep_re - 1.0) * lam_im) / denom
        keep_a = jnp.concatenate([keep_re, keep_re], axis=1)
        keep_b = jnp.concatenate([-keep_im, keep_im], axis=1)
        for i in range(5):
            loads[l, i].wait()
        for g in range(groups):
            t_re, t_im = b_re[l, g], b_im[l, g]
            r_re, r_im = ratio_re[g : g + 1, :], ratio_im[g : g + 1, :]
            drive[l, pl.ds(g * chans, chans), :] = jnp.concatenate(
                [r_re * t_re - r_im * t_im, r_re * t_im + r_im * t_re], axis=1
            )
        read[l] = jnp.concatenate([c_re[l].reshape(width, half), -c_im[l].reshape(width, half)], axis=1)
        for g in range(groups):
            old = state[l, pl.ds(g, rows_d, stride=groups), :]
            kept[l, pl.ds(g * rows_d, rows_d), :] = (
                keep_a[g : g + 1, :] * old + keep_b[g : g + 1, :] * pltpu.roll(old, lanes // 2, 1)
            )
        proj[...] = lax.dot_general(kept[l], read[l], NT, precision=HIGHEST, preferred_element_type=F32)
        total = jnp.zeros((rows_d, width), F32)
        for g in range(groups):
            total = jnp.where(lane_group == g, proj[pl.ds(g * rows_d, rows_d), :], total)
        from_old[l] = total
        full = lax.dot_general(drive[l], read[l], NT, precision=HIGHEST, preferred_element_type=F32)
        same = (
            lax.broadcasted_iota(jnp.int32, (width, width), 0) // chans
            == lax.broadcasted_iota(jnp.int32, (width, width), 1) // chans
        )
        mix_w[l] = jnp.where(same, full, 0.0)

    def update(l):
        u = u_keep[l]
        for g in range(groups):
            masked[pl.ds(g * rows_d, rows_d), :] = jnp.where(lane_group == g, u, 0.0)
        kept[l] = kept[l] + jnp.dot(masked[...], drive[l], precision=HIGHEST, preferred_element_type=F32)
        for g in range(groups):
            state[l, pl.ds(g, rows_d, stride=groups), :] = kept[l, pl.ds(g * rows_d, rows_d), :]

    pl.semaphore_wait(barrier, tp + dp - 2)
    for k in reversed(range(1, tp)):
        x_copy(0, k).start()
    x_all[0, me_t] = stream_ref[...]
    prepare(0)

    for l in range(layers):
        loads[l, 5].wait()
        gain = gain_ref[l : l + 1, :]
        own_part = own_sq = None
        for k in reversed(range(dp)):
            to = partner(me_d, k, dp)
            for j in range(per):
                t = to * per + j

                @pl.when(t != me_t)
                def _():
                    arrival(x_all.at[l, t], x_rs.at[l, t], "tp").wait_recv()

            x = x_all[l, pl.ds(to * per, per)].astype(F32).reshape(rows_d, feats)
            column = jnp.sum(x * x, axis=1, keepdims=True)
            squares = jnp.sum(jnp.where(eye, column, 0.0), axis=0, keepdims=True)
            product = jnp.dot((x * gain).astype(BF16), w_in[l], preferred_element_type=F32)
            if k:
                sq_send[l, to] = jnp.broadcast_to(squares, (8, sq_width))
                sq_copy(l, to).start()
                part_send[l, to] = product.astype(BF16)
                part_copy(l, to).start()
            else:
                own_part, own_sq = product, squares
        for k in range(1, dp):
            by = partner(me_d, k, dp, True)
            arrival(sq_recv.at[l, by], sq_rs.at[l, by], "dp").wait_recv()
            own_sq = own_sq + sq_recv[l, by][0:1, :]
            arrival(part_recv.at[l, by], part_rs.at[l, by], "dp").wait_recv()
            own_part = own_part + part_recv[l, by].astype(F32)
        square_total = jnp.sum(jnp.where(eye, own_sq, 0.0), axis=1, keepdims=True)
        u = lax.rsqrt(square_total / (feats * dp) + EPS) * own_part
        u_keep[l] = u
        pre = from_old[l] + jnp.dot(u, mix_w[l], precision=HIGHEST, preferred_element_type=F32) + skip_ref[l : l + 1, :] * u
        mix_all[l, me_d] = jax.nn.gelu(pre).astype(BF16)
        for k in reversed(range(1, dp)):
            mix_copy(l, partner(me_d, k, dp)).start()
        loads[l, 6].wait()
        loads[l, 7].wait()

        def pass_on(by):
            for m in range(per // 2):
                q = by * (per // 2) + m
                arrival(pair_recv.at[l, q], pair_rs.at[l, q], "tp").wait_recv()
                total = block[2 * q + side] + pair_recv[l, q].astype(F32)

                @pl.when(q != me_p)
                def _():
                    comb_send[l, 2 * q + side] = total.astype(BF16)
                    comb_copy(l, q).start()

                @pl.when(q == me_p)
                def _():
                    comb_own[...] = total

        for k in range(dp):
            by = partner(me_d, k, dp, True)
            if k:
                arrival(mix_all.at[l, by], mix_rs.at[l, by], "dp").wait_recv()
            mixed = mix_all[l, by]
            value = jnp.dot(mixed, w_val[l], preferred_element_type=F32)
            gate = jnp.dot(mixed, w_gate[l], preferred_element_type=F32)
            for j in range(per):
                rows = slice(j * rows_t, (j + 1) * rows_t)
                block[by * per + j, :, :feats] = value[rows]
                block[by * per + j, :, feats:] = gate[rows]
            for m in range(per // 2):
                q = by * (per // 2) + m
                comb_send[l, 2 * q + 1 - side] = block[2 * q + 1 - side].astype(BF16)
                pair_copy(l, q).start()
            if k > 1:
                pass_on(partner(me_d, k - 2, dp, True))
        for k in range(max(dp - 2, 0), dp):
            pass_on(partner(me_d, k, dp, True))

        update(l)
        if l + 1 < layers:
            prepare(l + 1)
        combined = comb_own[...]
        for k in range(1, tp // 2):
            by = partner(me_p, k, tp // 2, True)
            arrival(comb_recv.at[l, by], comb_rs.at[l, by], "tp").wait_recv()
            combined = combined + comb_recv[l, by].astype(F32)
        fresh = (
            x_all[l, me_t].astype(F32) + combined[:, :feats] * jax.nn.sigmoid(combined[:, feats:])
        ).astype(BF16)
        if l + 1 < layers:
            x_all[l + 1, me_t] = fresh
            for k in reversed(range(1, tp)):
                x_copy(l + 1, k).start()
        else:
            out_ref[...] = fresh

    for l in range(layers):
        for k in range(1, tp):
            x_copy(l, k).wait_send()
        for k in range(1, tp // 2):
            comb_copy(l, partner(me_p, k, tp // 2)).wait_send()
        for q in range(tp // 2):
            pair_copy(l, q).wait_send()
        for k in range(1, dp):
            to = partner(me_d, k, dp)
            part_copy(l, to).wait_send()
            sq_copy(l, to).wait_send()
            mix_copy(l, to).wait_send()


def per_device(
    tp, dp,
    stream, norm_gain, w_input, lam_re, lam_im, log_dt, b_re, b_im, readout_real, readout_imaginary, d_skip,
    w_val, w_gate, state,
):
    layers, feats, width = w_input.shape
    rows_t = stream.shape[0]
    rows_d, groups, lanes = state.shape[1:]
    chans = b_re.shape[-1]

    turned_re, turned_im = b_re.swapaxes(2, 3), b_im.swapaxes(2, 3)

    limit = 67043328 - 4 * layers * rows_d * groups * lanes - (256 << 10)
    vmem = pl.BlockSpec(memory_space=pltpu.VMEM)
    hbm = pl.BlockSpec(memory_space=pltpu.HBM)
    sq_width = max(rows_d, 128)
    dma = lambda *shape: pltpu.SemaphoreType.DMA(shape)
    out, states = pl.pallas_call(
        functools.partial(kernel, tp, dp, chans),
        out_shape=(pltpu.VMEM(stream.shape, BF16), pltpu.VMEM((layers, rows_d * groups, lanes), F32)),
        in_specs=[vmem, vmem, hbm, vmem, vmem, vmem, hbm, hbm, hbm, hbm, vmem, hbm, hbm, hbm],
        out_specs=(vmem, vmem),
        scratch_shapes=[
            pltpu.VMEM(w_input.shape, BF16),
            pltpu.VMEM(w_val.shape, BF16),
            pltpu.VMEM(w_gate.shape, BF16),
            pltpu.VMEM(turned_re.shape, F32),
            pltpu.VMEM(turned_im.shape, F32),
            pltpu.VMEM(readout_real.shape, F32),
            pltpu.VMEM(readout_imaginary.shape, F32),
            pltpu.VMEM((layers, width, lanes), F32),
            pltpu.VMEM((layers, width, lanes), F32),
            pltpu.VMEM((layers, rows_d * groups, lanes), F32),
            pltpu.VMEM((rows_d * groups, width), F32),
            pltpu.VMEM((layers, rows_d, width), F32),
            pltpu.VMEM((rows_d * groups, width), F32),
            pltpu.VMEM((layers, rows_d, width), F32),
            pltpu.VMEM((layers, width, width), F32),
            pltpu.VMEM((layers, tp, rows_t, feats), BF16),
            pltpu.VMEM((layers, dp, rows_d, width), BF16),
            pltpu.VMEM((layers, dp, rows_d, width), BF16),
            pltpu.VMEM((layers, dp, 8, sq_width), F32),
            pltpu.VMEM((layers, dp, 8, sq_width), F32),
            pltpu.VMEM((layers, dp, rows_d, width), BF16),
            pltpu.VMEM((tp, rows_t, 2 * feats), F32),
            pltpu.VMEM((layers, tp, rows_t, 2 * feats), BF16),
            pltpu.VMEM((rows_t, 2 * feats), F32),
            pltpu.VMEM((layers, tp // 2, rows_t, 2 * feats), BF16),
            pltpu.VMEM((layers, tp // 2, rows_t, 2 * feats), BF16),
            dma(layers, 8),
            dma(layers, tp), dma(layers, tp),
            dma(layers, dp), dma(layers, dp),
            dma(layers, dp), dma(layers, dp),
            dma(layers, dp), dma(layers, dp),
            dma(layers, tp // 2), dma(layers, tp // 2),
            dma(layers, tp // 2), dma(layers, tp // 2),
        ],
        compiler_params=pltpu.CompilerParams(collective_id=0, has_side_effects=True, vmem_limit_bytes=limit),
    )(
        stream, norm_gain, w_input, lam_re, lam_im, log_dt, turned_re, turned_im, readout_real,
        readout_imaginary, d_skip, w_val, w_gate,
        state.reshape(layers, rows_d * groups, lanes),
    )
    return out, states.reshape(state.shape)


def solution(mesh):
    return jax.shard_map(
        functools.partial(per_device, mesh.shape["tp"], mesh.shape["dp"]),
        mesh=mesh,
        in_specs=(
            P("tp", "dp"),
            P(None, "dp"),
            P(None, "dp", "tp"),
            P(None, "tp", None),
            P(None, "tp", None),
            P(None, "tp"),
            P(None, "tp", None, None),
            P(None, "tp", None, None),
            P(None, "tp", None, None),
            P(None, "tp", None, None),
            P(None, "tp"),
            P(None, "tp", "dp"),
            P(None, "tp", "dp"),
            P(None, "dp", "tp", None),
        ),
        out_specs=(P("tp", "dp"), P(None, "dp", "tp", None)),
        check_vma=False,
    )
```

profile of v0, /device:TPU:2, one launch (start us, length us, event | category | flops | bytes accessed | tf_op | source)
XLA Modules:
  0.0 55.5 jit_solution(12178747258190127167)
XLA Ops:
  0.6 53.2 %shard_map.149 = (bf16[32,512]{1,0:T(8,128)(2,1)S(1)}, f32[2,1024,128]{2,1,0:T(8,128)S(1)}) custom-call(bf16[32,512]{1,0:T(8,128)(2,1)} %stream_ref.1, f32[2,512]{1,0:T(2,128)} %gain_ref.1, bf16[2,512,256]{2,1,0:T(8,128)(2,1)} %w_in_hbm.1, f32[2,16,64]{2,1,0:T(8,128)} %lam_re_ref.1, f32[2,16,64]{2,1,0:T(8,128)} %lam_im_ref.1, f32[2,16]{1,0:T(2,128)} %log_dt_ref.1, ...), custom_call_target="tpu_custom_call" | custom-call | tf_op jit(solution)/shard_map/pallas_call | solution.py:278
  53.9 0.6 %copy.18 = bf16[32,512]{1,0:T(8,128)(2,1)} copy(bf16[32,512]{1,0:T(8,128)(2,1)S(1)} %get-tuple-element.6) | data formatting | bytes 65536
  54.5 1.0 %copy.19 = f32[2,64,16,128]{3,2,1,0:T(8,128)} copy(f32[2,64,16,128]{3,2,1,0:T(8,128)S(1)} %bitcast.4) | data formatting | bytes 2097152
where the time goes:
time: 56.3 us; the launch traced here: 55.5 us
  Pallas kernels  53.2 us (94%)
  local copies, waits for them, and re-layouts  1.59 us (3%)
  between operations  0.64 us (1%)
    pallas_call x1, Pallas kernels, per_device(): pl.pallas_call(functools.partial(kernel, tp, dp, chans), out_shape=(pltpu...  53.2 us
    unnamed x2, local copies, waits for them, and re-layouts  1.59 us

commit v1 on v0

--- a/solution.py
+++ b/solution.py
@@ -30,12 +30,12 @@
     stream_ref, gain_ref, w_in_hbm, lam_re_ref, lam_im_ref, log_dt_ref, b_re_hbm, b_im_hbm, c_re_hbm, c_im_hbm, skip_ref,
     w_val_hbm, w_gate_hbm, state_hbm,
     out_ref, state,
-    w_in, w_val, w_gate, b_re, b_im, c_re, c_im, drive, read,
+    gains, w_in, w_wide, w_val, w_gate, b_re, b_im, c_re, c_im, drive, read,
     kept, proj, u_keep, masked, from_old, mix_w,
-    x_all, part_send, part_recv, sq_send, sq_recv, mix_all, block, comb_send, comb_own, pair_recv, comb_recv,
-    load_sem, x_ss, x_rs, part_ss, part_rs, sq_ss, sq_rs, mix_ss, mix_rs, pair_ss, pair_rs, comb_ss, comb_rs,
+    x_own, x_all, x_wide, part_send, part_recv, sq_send, sq_recv, mix_all, block, comb_send, comb_own, pair_recv, comb_recv,
+    load_sem, gain_ss, gain_rs, give_ss, give_rs, pass_ss, x_ss, x_rs, part_ss, part_rs, sq_ss, sq_rs, mix_ss, mix_rs, pair_ss, pair_rs, comb_ss, comb_rs,
 ):
-    layers = w_in.shape[0]
+    layers = b_re.shape[0]
     me_t, me_d = lax.axis_index("tp"), lax.axis_index("dp")
     rows_t, feats = stream_ref.shape
     rows_d, width = u_keep.shape[1:]
@@ -43,7 +43,9 @@
     me_p, side = me_t // 2, me_t % 2
     groups, half = lam_re_ref.shape[1:]
     lanes = state.shape[2]
-    sq_width = sq_send.shape[3]
+    sq_width = sq_send.shape[2]
+    me_x, core, home = me_d // 2, me_d % 2, me_t // per
+    mate = 2 * me_x + 1 - core
 
     loads = {}
     for l in range(layers):
@@ -53,7 +55,8 @@
                 (w_in_hbm, w_in), (w_val_hbm, w_val), (w_gate_hbm, w_gate),
             )
         ):
-            loads[l, i] = pltpu.make_async_copy(src.at[l], dst.at[l], load_sem.at[l, i])
+            to = dst.at[l] if i != 5 else w_wide.at[l - 1, me_d] if l else w_in
+            loads[l, i] = pltpu.make_async_copy(src.at[l], to, load_sem.at[l, i])
             loads[l, i].start()
 
     barrier = pltpu.get_barrier_semaphore()
@@ -68,15 +71,32 @@
         )
 
     def x_copy(l, k):
-        src = stream_ref if l == 0 else x_all.at[l, me_t]
         to = partner(me_t, k, tp)
-        return send(src, x_all.at[l, me_t], x_ss.at[l, to], x_rs.at[l, me_t], "tp", to)
-
-    def part_copy(l, to):
-        return send(part_send.at[l, to], part_recv.at[l, me_d], part_ss.at[l, to], part_rs.at[l, me_d], "dp", to)
-
-    def sq_copy(l, to):
-        return send(sq_send.at[l, to], sq_recv.at[l, me_d], sq_ss.at[l, to], sq_rs.at[l, me_d], "dp", to)
+        if l == 0:
+            return send(stream_ref, x_all.at[me_t], x_ss.at[l, to], x_rs.at[l, me_t], "tp", to)
+        slot = me_t % per
+        return pltpu.make_async_remote_copy(
+            src_ref=x_own.at[l - 1], dst_ref=x_wide.at[l - 1, me_d, slot], send_sem=x_ss.at[l, to],
+            recv_sem=x_rs.at[l, me_d * per + slot], device_id={"tp": to, "dp": home}, device_id_type=pl.DeviceIdType.MESH,
+        )
+
+    def gain_copy(to):
+        return send(gain_ref, gains.at[me_d], gain_ss.at[to], gain_rs.at[me_d], "dp", to)
+
+    def give_copy(l, to):
+        return send(w_in_hbm.at[l], w_wide.at[l - 1, me_d], give_ss.at[l - 1, to], give_rs.at[l - 1, me_d], "dp", to)
+
+    def pass_copy(l, block):
+        ref = w_wide.at[l - 1, block]
+        return send(ref, ref, pass_ss.at[l - 1, block], give_rs.at[l - 1, block], "dp", mate)
+
+    far = [2 * partner(me_x, k, dp // 2) + core for k in range(1, dp // 2)]
+
+    def part_copy(to):
+        return send(part_send.at[to], part_recv.at[me_d], part_ss.at[to], part_rs.at[me_d], "dp", to)
+
+    def sq_copy(to):
+        return send(sq_send.at[to], sq_recv.at[me_d], sq_ss.at[to], sq_rs.at[me_d], "dp", to)
 
     def mix_copy(l, to):
         return send(mix_all.at[l, me_d], mix_all.at[l, me_d], mix_ss.at[l, to], mix_rs.at[l, me_d], "dp", to)
@@ -148,46 +168,75 @@
     pl.semaphore_wait(barrier, tp + dp - 2)
     for k in reversed(range(1, tp)):
         x_copy(0, k).start()
-    x_all[0, me_t] = stream_ref[...]
+    for k in range(1, dp):
+        gain_copy(partner(me_d, k, dp)).start()
+    x_all[me_t] = stream_ref[...]
+    gains[me_d] = gain_ref[...]
     prepare(0)
 
     for l in range(layers):
         loads[l, 5].wait()
-        gain = gain_ref[l : l + 1, :]
-        own_part = own_sq = None
-        for k in reversed(range(dp)):
-            to = partner(me_d, k, dp)
-            for j in range(per):
-                t = to * per + j
-
-                @pl.when(t != me_t)
-                def _():
-                    arrival(x_all.at[l, t], x_rs.at[l, t], "tp").wait_recv()
-
-            x = x_all[l, pl.ds(to * per, per)].astype(F32).reshape(rows_d, feats)
-            column = jnp.sum(x * x, axis=1, keepdims=True)
-            squares = jnp.sum(jnp.where(eye, column, 0.0), axis=0, keepdims=True)
-            product = jnp.dot((x * gain).astype(BF16), w_in[l], preferred_element_type=F32)
-            if k:
-                sq_send[l, to] = jnp.broadcast_to(squares, (8, sq_width))
-                sq_copy(l, to).start()
-                part_send[l, to] = product.astype(BF16)
-                part_copy(l, to).start()
-            else:
-                own_part, own_sq = product, squares
-        for k in range(1, dp):
-            by = partner(me_d, k, dp, True)
-            arrival(sq_recv.at[l, by], sq_rs.at[l, by], "dp").wait_recv()
-            own_sq = own_sq + sq_recv[l, by][0:1, :]
-            arrival(part_recv.at[l, by], part_rs.at[l, by], "dp").wait_recv()
-            own_part = own_part + part_recv[l, by].astype(F32)
-        square_total = jnp.sum(jnp.where(eye, own_sq, 0.0), axis=1, keepdims=True)
+        if l == 0:
+            gain = gain_ref[l : l + 1, :]
+            own_part = own_sq = None
+            for k in reversed(range(dp)):
+                to = partner(me_d, k, dp)
+                for j in range(per):
+                    t = to * per + j
+
+                    @pl.when(t != me_t)
+                    def _():
+                        arrival(x_all.at[t], x_rs.at[l, t], "tp").wait_recv()
+
+                x = x_all[pl.ds(to * per, per)].astype(F32).reshape(rows_d, feats)
+                column = jnp.sum(x * x, axis=1, keepdims=True)
+                squares = jnp.sum(jnp.where(eye, column, 0.0), axis=0, keepdims=True)
+                product = jnp.dot((x * gain).astype(BF16), w_in[...], preferred_element_type=F32)
+                if k:
+                    sq_send[to] = jnp.broadcast_to(squares, (8, sq_width))
+                    sq_copy(to).start()
+                    part_send[to] = product.astype(BF16)
+                    part_copy(to).start()
+                else:
+                    own_part, own_sq = product, squares
+            for k in range(1, dp):
+                by = partner(me_d, k, dp, True)
+                arrival(sq_recv.at[by], sq_rs.at[by], "dp").wait_recv()
+                own_sq = own_sq + sq_recv[by][0:1, :]
+                arrival(part_recv.at[by], part_rs.at[by], "dp").wait_recv()
+                own_part = own_part + part_recv[by].astype(F32)
+            square_total = jnp.sum(jnp.where(eye, own_sq, 0.0), axis=1, keepdims=True)
+        else:
+            own_part = square_total = 0.0
+            for k in range(dp):
+                by = partner(me_d, k, dp, True)
+                if k:
+                    if l == 1:
+                        arrival(gains.at[by], gain_rs.at[by], "dp").wait_recv()
+
+                    @pl.when(by % 2 != core)
+                    def _():
+                        arrival(w_wide.at[l - 1, by], give_rs.at[l - 1, by], "dp").wait_recv()
+
+                for j in range(per):
+
+                    @pl.when((me_d * per + j != me_t) | (by != me_d))
+                    def _():
+                        arrival(x_wide.at[l - 1, by, j], x_rs.at[l, by * per + j], "tp").wait_recv()
+
+                x = x_wide[l - 1, by].astype(F32).reshape(rows_d, feats)
+                square_total = square_total + jnp.sum(x * x, axis=1, keepdims=True)
+                normed = (x * gains[by, l : l + 1, :]).astype(BF16)
+                own_part = own_part + jnp.dot(normed, w_wide[l - 1, by], preferred_element_type=F32)
         u = lax.rsqrt(square_total / (feats * dp) + EPS) * own_part
         u_keep[l] = u
         pre = from_old[l] + jnp.dot(u, mix_w[l], precision=HIGHEST, preferred_element_type=F32) + skip_ref[l : l + 1, :] * u
         mix_all[l, me_d] = jax.nn.gelu(pre).astype(BF16)
         for k in reversed(range(1, dp)):
             mix_copy(l, partner(me_d, k, dp)).start()
+        if l + 1 < layers:
+            for to in (*far, mate):
+                give_copy(l + 1, to).start()
         loads[l, 6].wait()
         loads[l, 7].wait()
 
@@ -229,33 +278,62 @@
         update(l)
         if l + 1 < layers:
             prepare(l + 1)
+            for owner in far:
+                arrival(w_wide.at[l, owner], give_rs.at[l, owner], "dp").wait_recv()
+                pass_copy(l + 1, owner).start()
         combined = comb_own[...]
         for k in range(1, tp // 2):
             by = partner(me_p, k, tp // 2, True)
             arrival(comb_recv.at[l, by], comb_rs.at[l, by], "tp").wait_recv()
             combined = combined + comb_recv[l, by].astype(F32)
-        fresh = (
-            x_all[l, me_t].astype(F32) + combined[:, :feats] * jax.nn.sigmoid(combined[:, feats:])
-        ).astype(BF16)
+        old = x_own[l - 1] if l else stream_ref[...]
+        fresh = (old.astype(F32) + combined[:, :feats] * jax.nn.sigmoid(combined[:, feats:])).astype(BF16)
         if l + 1 < layers:
-            x_all[l + 1, me_t] = fresh
+            x_own[l] = fresh
             for k in reversed(range(1, tp)):
                 x_copy(l + 1, k).start()
+            pl.when(home != me_d)(lambda: x_copy(l + 1, 0).start())
+
+            @pl.when(home == me_d)
+            def _():
+                x_wide[l, me_d, me_t % per] = fresh
         else:
             out_ref[...] = fresh
 
     for l in range(layers):
         for k in range(1, tp):
             x_copy(l, k).wait_send()
+        if l:
+            pl.when(home != me_d)(lambda: x_copy(l, 0).wait_send())
+            for to in (*far, mate):
+                give_copy(l, to).wait_send()
+            for owner in far:
+                pass_copy(l, owner).wait_send()
         for k in range(1, tp // 2):
             comb_copy(l, partner(me_p, k, tp // 2)).wait_send()
         for q in range(tp // 2):
             pair_copy(l, q).wait_send()
         for k in range(1, dp):
-            to = partner(me_d, k, dp)
-            part_copy(l, to).wait_send()
-            sq_copy(l, to).wait_send()
-            mix_copy(l, to).wait_send()
+            mix_copy(l, partner(me_d, k, dp)).wait_send()
+    for k in range(1, dp):
+        to = partner(me_d, k, dp)
+        gain_copy(to).wait_send()
+        part_copy(to).wait_send()
+        sq_copy(to).wait_send()
+
+
+def store(x_ref, state_ref, x_out, state_out, sem):
+    middle = state_ref.shape[0] // 2
+    first, second = pl.ds(0, middle), pl.ds(middle, state_ref.shape[0] - middle)
+    copies = [
+        pltpu.make_async_copy(state_ref.at[first], state_out.at[first], sem.at[0]),
+        pltpu.make_async_copy(state_ref.at[second], state_out.at[second], sem.at[1]),
+        pltpu.make_async_copy(x_ref, x_out, sem.at[2]),
+    ]
+    for copy in copies:
+        copy.start()
+    for copy in copies:
+        copy.wait()
 
 
 def per_device(
@@ -281,7 +359,9 @@
         in_specs=[vmem, vmem, hbm, vmem, vmem, vmem, hbm, hbm, hbm, hbm, vmem, hbm, hbm, hbm],
         out_specs=(vmem, vmem),
         scratch_shapes=[
-            pltpu.VMEM(w_input.shape, BF16),
+            pltpu.VMEM((dp, layers, feats), F32),
+            pltpu.VMEM((feats, width), BF16),
+            pltpu.VMEM((layers - 1, dp, feats, width), BF16),
             pltpu.VMEM(w_val.shape, BF16),
             pltpu.VMEM(w_gate.shape, BF16),
             pltpu.VMEM(turned_re.shape, F32),
@@ -296,11 +376,13 @@
             pltpu.VMEM((rows_d * groups, width), F32),
             pltpu.VMEM((layers, rows_d, width), F32),
             pltpu.VMEM((layers, width, width), F32),
-            pltpu.VMEM((layers, tp, rows_t, feats), BF16),
-            pltpu.VMEM((layers, dp, rows_d, width), BF16),
-            pltpu.VMEM((layers, dp, rows_d, width), BF16),
-            pltpu.VMEM((layers, dp, 8, sq_width), F32),
-            pltpu.VMEM((layers, dp, 8, sq_width), F32),
+            pltpu.VMEM((layers - 1, rows_t, feats), BF16),
+            pltpu.VMEM((tp, rows_t, feats), BF16),
+            pltpu.VMEM((layers - 1, dp, rows_d // rows_t, rows_t, feats), BF16),
+            pltpu.VMEM((dp, rows_d, width), BF16),
+            pltpu.VMEM((dp, rows_d, width), BF16),
+            pltpu.VMEM((dp, 8, sq_width), F32),
+            pltpu.VMEM((dp, 8, sq_width), F32),
             pltpu.VMEM((layers, dp, rows_d, width), BF16),
             pltpu.VMEM((tp, rows_t, 2 * feats), F32),
             pltpu.VMEM((layers, tp, rows_t, 2 * feats), BF16),
@@ -308,9 +390,11 @@
             pltpu.VMEM((layers, tp // 2, rows_t, 2 * feats), BF16),
             pltpu.VMEM((layers, tp // 2, rows_t, 2 * feats), BF16),
             dma(layers, 8),
+            dma(dp), dma(dp),
+            dma(layers - 1, dp), dma(layers - 1, dp), dma(layers - 1, dp),
             dma(layers, tp), dma(layers, tp),
-            dma(layers, dp), dma(layers, dp),
-            dma(layers, dp), dma(layers, dp),
+            dma(dp), dma(dp),
+            dma(dp), dma(dp),
             dma(layers, dp), dma(layers, dp),
             dma(layers, tp // 2), dma(layers, tp // 2),
             dma(layers, tp // 2), dma(layers, tp // 2),
@@ -321,6 +405,14 @@
         readout_imaginary, d_skip, w_val, w_gate,
         state.reshape(layers, rows_d * groups, lanes),
     )
+    hbm_out = lambda a: jax.ShapeDtypeStruct(a.shape, a.dtype)
+    out, states = pl.pallas_call(
+        store,
+        out_shape=(hbm_out(stream), jax.ShapeDtypeStruct((layers, rows_d * groups, lanes), F32)),
+        in_specs=[vmem, vmem],
+        out_specs=(hbm, hbm),
+        scratch_shapes=[dma(3)],
+    )(*(pltpu.with_memory_space_constraint(a, pltpu.VMEM) for a in (out, states)))
     return out, states.reshape(state.shape)
 
 

time: 56.3 us -> 52.1 us (0.925)
  Pallas kernels: 53.2 us -> 50.7 us
  local copies, waits for them, and re-layouts: 1.59 us -> 0 us
    pallas_call x1, Pallas kernels: 53.2 us -> 49.7 us  [per_device(): pl.pallas_call(functools.partial(kernel, tp, dp, chans), out_shape=(pltpu...]
    unnamed x2 -> x0, local copies, waits for them, and re-layouts: 1.59 us -> none
    pallas_call x0 -> x1, Pallas kernels: none -> 1 us  [per_device(): pl.pallas_call(store, out_shape=(hbm_out(stream), jax.ShapeDtypeStruct((l...]
where the time goes in v1:
time: 52.1 us; the launch traced here: 51.3 us
  Pallas kernels  50.7 us (97%)
  between operations  0.64 us (1%)
    pallas_call x1, Pallas kernels, per_device(): pl.pallas_call(functools.partial(kernel, tp, dp, chans), out_shape=(pltpu...  49.7 us

profile of v1, /device:TPU:2, one launch (start us, length us, event | category | flops | bytes accessed | tf_op | source)
XLA Modules:
  0.0 51.3 jit_solution(4216447081940152414)
XLA Ops:
  0.6 49.7 %shard_map.149 = (bf16[32,512]{1,0:T(8,128)(2,1)S(1)}, f32[2,1024,128]{2,1,0:T(8,128)S(1)}) custom-call(bf16[32,512]{1,0:T(8,128)(2,1)} %stream_ref.1, f32[2,512]{1,0:T(2,128)} %gain_ref.1, bf16[2,512,256]{2,1,0:T(8,128)(2,1)} %w_in_hbm.1, f32[2,16,64]{2,1,0:T(8,128)} %lam_re_ref.1, f32[2,16,64]{2,1,0:T(8,128)} %lam_im_ref.1, f32[2,16]{1,0:T(2,128)} %log_dt_ref.1, ...), custom_call_target="tpu_custom_call" | custom-call | tf_op jit(solution)/shard_map/pallas_call | solution.py:356
  50.3 1.0 %shard_map.150 = (bf16[32,512]{1,0:T(8,128)(2,1)}, f32[2,1024,128]{2,1,0:T(8,128)}) custom-call(bf16[32,512]{1,0:T(8,128)(2,1)S(1)} %get-tuple-element.6.x_ref, f32[2,1024,128]{2,1,0:T(8,128)S(1)} %get-tuple-element.7.state_ref), custom_call_target="tpu_custom_call" | custom-call | tf_op jit(solution)/shard_map/pallas_call | solution.py:409

commit v2 on v1

--- a/solution.py
+++ b/solution.py
@@ -27,13 +27,14 @@
 
 def kernel(
     tp, dp, chans,
-    stream_ref, gain_ref, w_in_hbm, lam_re_ref, lam_im_ref, log_dt_ref, b_re_hbm, b_im_hbm, c_re_hbm, c_im_hbm, skip_ref,
+    stream_hbm, gain_hbm, w_in_hbm, lam_re_hbm, lam_im_hbm, log_dt_hbm, b_re_hbm, b_im_hbm, c_re_hbm, c_im_hbm, skip_hbm,
     w_val_hbm, w_gate_hbm, state_hbm,
     out_ref, state,
+    stream_ref, gain_ref, lam_re_ref, lam_im_ref, log_dt_ref, skip_ref,
     gains, w_in, w_wide, w_val, w_gate, b_re, b_im, c_re, c_im, drive, read,
     kept, proj, u_keep, masked, from_old, mix_w,
-    x_own, x_all, x_wide, part_send, part_recv, sq_send, sq_recv, mix_all, block, comb_send, comb_own, pair_recv, comb_recv,
-    load_sem, gain_ss, gain_rs, give_ss, give_rs, pass_ss, x_ss, x_rs, part_ss, part_rs, sq_ss, sq_rs, mix_ss, mix_rs, pair_ss, pair_rs, comb_ss, comb_rs,
+    x_own, x_all, x_wide, x_rest, part_send, part_recv, sq_send, sq_recv, mix_all, block, comb_send, comb_own, pair_recv, comb_recv,
+    small_sem, load_sem, gain_ss, gain_rs, give_ss, give_rs, pass_ss, rest_ss, rest_rs, x_ss, x_rs, part_ss, part_rs, sq_ss, sq_rs, mix_ss, mix_rs, pair_ss, pair_rs, comb_ss, comb_rs,
 ):
     layers = b_re.shape[0]
     me_t, me_d = lax.axis_index("tp"), lax.axis_index("dp")
@@ -46,7 +47,28 @@
     sq_width = sq_send.shape[2]
     me_x, core, home = me_d // 2, me_d % 2, me_t // per
     mate = 2 * me_x + 1 - core
-
+    halves, pairs = dp // 2, per // 2
+    spread = lambda block: block % 2 * halves + block // 2
+    held = home % halves * 2 + home // halves
+    final = held * per + me_t % per
+
+    barrier = pltpu.get_barrier_semaphore()
+    for k in range(1, dp):
+        pl.semaphore_signal(barrier, inc=1, device_id={"dp": partner(me_d, k, dp)}, device_id_type=pl.DeviceIdType.MESH)
+    for k in range(1, tp):
+        pl.semaphore_signal(barrier, inc=1, device_id={"tp": partner(me_t, k, tp)}, device_id_type=pl.DeviceIdType.MESH)
+
+    small = [
+        pltpu.make_async_copy(src, dst, small_sem.at[i])
+        for i, (src, dst) in enumerate(
+            (
+                (stream_hbm, stream_ref), (gain_hbm, gain_ref), (lam_re_hbm, lam_re_ref), (lam_im_hbm, lam_im_ref),
+                (log_dt_hbm, log_dt_ref), (skip_hbm, skip_ref),
+            )
+        )
+    ]
+    for copy in small:
+        copy.start()
     loads = {}
     for l in range(layers):
         for i, (src, dst) in enumerate(
@@ -59,12 +81,6 @@
             loads[l, i] = pltpu.make_async_copy(src.at[l], to, load_sem.at[l, i])
             loads[l, i].start()
 
-    barrier = pltpu.get_barrier_semaphore()
-    for k in range(1, dp):
-        pl.semaphore_signal(barrier, inc=1, device_id={"dp": partner(me_d, k, dp)}, device_id_type=pl.DeviceIdType.MESH)
-    for k in range(1, tp):
-        pl.semaphore_signal(barrier, inc=1, device_id={"tp": partner(me_t, k, tp)}, device_id_type=pl.DeviceIdType.MESH)
-
     def send(src, dst, ss, rs, axis, to):
         return pltpu.make_async_remote_copy(
             src_ref=src, dst_ref=dst, send_sem=ss, recv_sem=rs, device_id={axis: to}, device_id_type=pl.DeviceIdType.MESH
@@ -77,8 +93,11 @@
         slot = me_t % per
         return pltpu.make_async_remote_copy(
             src_ref=x_own.at[l - 1], dst_ref=x_wide.at[l - 1, me_d, slot], send_sem=x_ss.at[l, to],
-            recv_sem=x_rs.at[l, me_d * per + slot], device_id={"tp": to, "dp": home}, device_id_type=pl.DeviceIdType.MESH,
-        )
+            recv_sem=x_rs.at[l, me_d * per + slot], device_id={"tp": to, "dp": held}, device_id_type=pl.DeviceIdType.MESH,
+        )
+
+    def rest_copy():
+        return send(x_own.at[layers - 2], x_rest, rest_ss.at[0], rest_rs.at[0], "tp", final)
 
     def gain_copy(to):
         return send(gain_ref, gains.at[me_d], gain_ss.at[to], gain_rs.at[me_d], "dp", to)
@@ -101,14 +120,14 @@
     def mix_copy(l, to):
         return send(mix_all.at[l, me_d], mix_all.at[l, me_d], mix_ss.at[l, to], mix_rs.at[l, me_d], "dp", to)
 
-    def comb_copy(l, to):
+    def comb_copy(l, r, to):
         return send(
-            comb_send.at[l, 2 * to + side], comb_recv.at[l, me_p], comb_ss.at[l, to], comb_rs.at[l, me_p], "tp", 2 * to + side
-        )
-
-    def pair_copy(l, q):
+            comb_send.at[l, 2 * r + side], comb_recv.at[l, me_p], comb_ss.at[l, to], comb_rs.at[l, me_p], "tp", 2 * to + side
+        )
+
+    def pair_copy(l, r):
         return send(
-            comb_send.at[l, 2 * q + 1 - side], pair_recv.at[l, q], pair_ss.at[l, q], pair_rs.at[l, q], "tp", 2 * me_p + 1 - side
+            comb_send.at[l, 2 * r + 1 - side], pair_recv.at[l, r], pair_ss.at[l, r], pair_rs.at[l, r], "tp", 2 * me_p + 1 - side
         )
 
     def arrival(ref, rs, axis):
@@ -165,6 +184,8 @@
         for g in range(groups):
             state[l, pl.ds(g, rows_d, stride=groups), :] = kept[l, pl.ds(g * rows_d, rows_d), :]
 
+    small[0].wait()
+    small[1].wait()
     pl.semaphore_wait(barrier, tp + dp - 2)
     for k in reversed(range(1, tp)):
         x_copy(0, k).start()
@@ -172,6 +193,8 @@
         gain_copy(partner(me_d, k, dp)).start()
     x_all[me_t] = stream_ref[...]
     gains[me_d] = gain_ref[...]
+    for copy in small[2:]:
+        copy.wait()
     prepare(0)
 
     for l in range(layers):
@@ -220,7 +243,7 @@
 
                 for j in range(per):
 
-                    @pl.when((me_d * per + j != me_t) | (by != me_d))
+                    @pl.when((spread(me_d) * per + j != me_t) | (by != me_d))
                     def _():
                         arrival(x_wide.at[l - 1, by, j], x_rs.at[l, by * per + j], "tp").wait_recv()
 
@@ -241,15 +264,16 @@
         loads[l, 7].wait()
 
         def pass_on(by):
-            for m in range(per // 2):
-                q = by * (per // 2) + m
-                arrival(pair_recv.at[l, q], pair_rs.at[l, q], "tp").wait_recv()
-                total = block[2 * q + side] + pair_recv[l, q].astype(F32)
+            for m in range(pairs):
+                r = by * pairs + m
+                q = (spread(by) if l + 1 < layers else by) * pairs + m
+                arrival(pair_recv.at[l, r], pair_rs.at[l, r], "tp").wait_recv()
+                total = block[2 * r + side] + pair_recv[l, r].astype(F32)
 
                 @pl.when(q != me_p)
                 def _():
-                    comb_send[l, 2 * q + side] = total.astype(BF16)
-                    comb_copy(l, q).start()
+                    comb_send[l, 2 * r + side] = total.astype(BF16)
+                    comb_copy(l, r, q).start()
 
                 @pl.when(q == me_p)
                 def _():
@@ -266,16 +290,17 @@
                 rows = slice(j * rows_t, (j + 1) * rows_t)
                 block[by * per + j, :, :feats] = value[rows]
                 block[by * per + j, :, feats:] = gate[rows]
-            for m in range(per // 2):
-                q = by * (per // 2) + m
-                comb_send[l, 2 * q + 1 - side] = block[2 * q + 1 - side].astype(BF16)
-                pair_copy(l, q).start()
+            for m in range(pairs):
+                r = by * pairs + m
+                comb_send[l, 2 * r + 1 - side] = block[2 * r + 1 - side].astype(BF16)
+                pair_copy(l, r).start()
             if k > 1:
                 pass_on(partner(me_d, k - 2, dp, True))
         for k in range(max(dp - 2, 0), dp):
             pass_on(partner(me_d, k, dp, True))
 
-        update(l)
+        if l + 1 == layers:
+            update(l)
         if l + 1 < layers:
             prepare(l + 1)
             for owner in far:
@@ -286,17 +311,32 @@
             by = partner(me_p, k, tp // 2, True)
             arrival(comb_recv.at[l, by], comb_rs.at[l, by], "tp").wait_recv()
             combined = combined + comb_recv[l, by].astype(F32)
-        old = x_own[l - 1] if l else stream_ref[...]
+        if l == 0:
+            old = x_all[final]
+        elif l + 1 < layers:
+            old = x_own[l - 1]
+        else:
+            pl.when(held != home)(lambda: arrival(x_rest, rest_rs.at[0], "tp").wait_recv())
+            old = x_rest[...]
         fresh = (old.astype(F32) + combined[:, :feats] * jax.nn.sigmoid(combined[:, feats:])).astype(BF16)
         if l + 1 < layers:
             x_own[l] = fresh
             for k in reversed(range(1, tp)):
                 x_copy(l + 1, k).start()
-            pl.when(home != me_d)(lambda: x_copy(l + 1, 0).start())
-
-            @pl.when(home == me_d)
+            pl.when(held != me_d)(lambda: x_copy(l + 1, 0).start())
+
+            @pl.when(held == me_d)
             def _():
                 x_wide[l, me_d, me_t % per] = fresh
+
+            if l + 2 == layers:
+                pl.when(held != home)(lambda: rest_copy().start())
+
+                @pl.when(held == home)
+                def _():
+                    x_rest[...] = fresh
+
+            update(l)
         else:
             out_ref[...] = fresh
 
@@ -304,17 +344,18 @@
         for k in range(1, tp):
             x_copy(l, k).wait_send()
         if l:
-            pl.when(home != me_d)(lambda: x_copy(l, 0).wait_send())
+            pl.when(held != me_d)(lambda: x_copy(l, 0).wait_send())
             for to in (*far, mate):
                 give_copy(l, to).wait_send()
             for owner in far:
                 pass_copy(l, owner).wait_send()
         for k in range(1, tp // 2):
-            comb_copy(l, partner(me_p, k, tp // 2)).wait_send()
+            comb_copy(l, 0, partner(me_p, k, tp // 2)).wait_send()
         for q in range(tp // 2):
             pair_copy(l, q).wait_send()
         for k in range(1, dp):
             mix_copy(l, partner(me_d, k, dp)).wait_send()
+    pl.when(held != home)(lambda: rest_copy().wait_send())
     for k in range(1, dp):
         to = partner(me_d, k, dp)
         gain_copy(to).wait_send()
@@ -356,9 +397,11 @@
     out, states = pl.pallas_call(
         functools.partial(kernel, tp, dp, chans),
         out_shape=(pltpu.VMEM(stream.shape, BF16), pltpu.VMEM((layers, rows_d * groups, lanes), F32)),
-        in_specs=[vmem, vmem, hbm, vmem, vmem, vmem, hbm, hbm, hbm, hbm, vmem, hbm, hbm, hbm],
+        in_specs=[hbm] * 14,
         out_specs=(vmem, vmem),
         scratch_shapes=[
+            pltpu.VMEM(stream.shape, BF16),
+            *(pltpu.VMEM(a.shape, F32) for a in (norm_gain, lam_re, lam_im, log_dt, d_skip)),
             pltpu.VMEM((dp, layers, feats), F32),
             pltpu.VMEM((feats, width), BF16),
             pltpu.VMEM((layers - 1, dp, feats, width), BF16),
@@ -379,6 +422,7 @@
             pltpu.VMEM((layers - 1, rows_t, feats), BF16),
             pltpu.VMEM((tp, rows_t, feats), BF16),
             pltpu.VMEM((layers - 1, dp, rows_d // rows_t, rows_t, feats), BF16),
+            pltpu.VMEM(stream.shape, BF16),
             pltpu.VMEM((dp, rows_d, width), BF16),
             pltpu.VMEM((dp, rows_d, width), BF16),
             pltpu.VMEM((dp, 8, sq_width), F32),
@@ -389,9 +433,11 @@
             pltpu.VMEM((rows_t, 2 * feats), F32),
             pltpu.VMEM((layers, tp // 2, rows_t, 2 * feats), BF16),
             pltpu.VMEM((layers, tp // 2, rows_t, 2 * feats), BF16),
+            dma(6),
             dma(layers, 8),
             dma(dp), dma(dp),
             dma(layers - 1, dp), dma(layers - 1, dp), dma(layers - 1, dp),
+            dma(1), dma(1),
             dma(layers, tp), dma(layers, tp),
             dma(dp), dma(dp),
             dma(dp), dma(dp),

time: 52.1 us -> 49.7 us (0.954); the launches traced: 51.3 us -> 49.6 us
  Pallas kernels: 50.7 us -> 49 us
    pallas_call x1, Pallas kernels: 49.7 us -> 48 us  [per_device(): pl.pallas_call(functools.partial(kernel, tp, dp, chans), out_shape=(pltpu...]
where the time goes in v2:
time: 49.7 us; the launch traced here: 49.6 us
  Pallas kernels  49 us (99%)
  between operations  0.64 us (1%)
    pallas_call x1, Pallas kernels, per_device(): pl.pallas_call(functools.partial(kernel, tp, dp, chans), out_shape=(pltpu...  48 us
    pallas_call x1, Pallas kernels, per_device(): pl.pallas_call(store, out_shape=(hbm_out(stream), jax.ShapeDtypeStruct((l...  1 us

profile of v2, /device:TPU:2, one launch (start us, length us, event | category | flops | bytes accessed | tf_op | source)
XLA Modules:
  0.0 49.6 jit_solution(9632391311451331214)
XLA Ops:
  0.6 48.0 %shard_map.149 = (bf16[32,512]{1,0:T(8,128)(2,1)S(1)}, f32[2,1024,128]{2,1,0:T(8,128)S(1)}) custom-call(bf16[32,512]{1,0:T(8,128)(2,1)} %stream_hbm.1, f32[2,512]{1,0:T(2,128)} %gain_hbm.1, bf16[2,512,256]{2,1,0:T(8,128)(2,1)} %w_in_hbm.1, f32[2,16,64]{2,1,0:T(8,128)} %lam_re_hbm.1, f32[2,16,64]{2,1,0:T(8,128)} %lam_im_hbm.1, f32[2,16]{1,0:T(2,128)} %log_dt_hbm.1, ...), custom_call_target="tpu_custom_call" | custom-call | tf_op jit(solution)/shard_map/pallas_call | solution.py:397
  48.6 1.0 %shard_map.150 = (bf16[32,512]{1,0:T(8,128)(2,1)}, f32[2,1024,128]{2,1,0:T(8,128)}) custom-call(bf16[32,512]{1,0:T(8,128)(2,1)S(1)} %get-tuple-element.6.x_ref, f32[2,1024,128]{2,1,0:T(8,128)S(1)} %get-tuple-element.7.state_ref), custom_call_target="tpu_custom_call" | custom-call | tf_op jit(solution)/shard_map/pallas_call | solution.py:455

commit v3 on v2

--- a/solution.py
+++ b/solution.py
@@ -34,7 +34,7 @@
     gains, w_in, w_wide, w_val, w_gate, b_re, b_im, c_re, c_im, drive, read,
     kept, proj, u_keep, masked, from_old, mix_w,
     x_own, x_all, x_wide, x_rest, part_send, part_recv, sq_send, sq_recv, mix_all, block, comb_send, comb_own, pair_recv, comb_recv,
-    small_sem, load_sem, gain_ss, gain_rs, give_ss, give_rs, pass_ss, rest_ss, rest_rs, x_ss, x_rs, part_ss, part_rs, sq_ss, sq_rs, mix_ss, mix_rs, pair_ss, pair_rs, comb_ss, comb_rs,
+    small_sem, load_sem, gain_ss, gain_rs, give_ss, give_rs, pass_ss, relay_ss, rest_ss, rest_rs, x_ss, x_rs, part_ss, part_rs, sq_ss, sq_rs, mix_ss, mix_rs, pair_ss, pair_rs, comb_ss, comb_rs,
 ):
     layers = b_re.shape[0]
     me_t, me_d = lax.axis_index("tp"), lax.axis_index("dp")
@@ -47,7 +47,7 @@
     sq_width = sq_send.shape[2]
     me_x, core, home = me_d // 2, me_d % 2, me_t // per
     mate = 2 * me_x + 1 - core
-    halves, pairs = dp // 2, per // 2
+    halves, pairs, quads = dp // 2, per // 2, tp // 2
     spread = lambda block: block % 2 * halves + block // 2
     held = home % halves * 2 + home // halves
     final = held * per + me_t % per
@@ -95,6 +95,17 @@
             src_ref=x_own.at[l - 1], dst_ref=x_wide.at[l - 1, me_d, slot], send_sem=x_ss.at[l, to],
             recv_sem=x_rs.at[l, me_d * per + slot], device_id={"tp": to, "dp": held}, device_id_type=pl.DeviceIdType.MESH,
         )
+
+    ends = quads - 1
+    relay = (me_p == 1) | (me_p == ends - 1)
+    origin = jnp.where(me_p == 1, ends, 0)
+
+    def distant(to):
+        return (jnp.abs(me_p - to // 2) == ends) & (ends > 2)
+
+    def relay_copy(j):
+        t = 2 * origin + j
+        return send(x_all.at[t], x_all.at[t], relay_ss.at[j], x_rs.at[0, t], "tp", 2 * (ends - origin) + side)
 
     def rest_copy():
         return send(x_own.at[layers - 2], x_rest, rest_ss.at[0], rest_rs.at[0], "tp", final)
@@ -188,7 +199,7 @@
     small[1].wait()
     pl.semaphore_wait(barrier, tp + dp - 2)
     for k in reversed(range(1, tp)):
-        x_copy(0, k).start()
+        pl.when(jnp.logical_not(distant(partner(me_t, k, tp))))(lambda: x_copy(0, k).start())
     for k in range(1, dp):
         gain_copy(partner(me_d, k, dp)).start()
     x_all[me_t] = stream_ref[...]
@@ -202,12 +213,20 @@
         if l == 0:
             gain = gain_ref[l : l + 1, :]
             own_part = own_sq = None
+            if quads > 3:
+
+                @pl.when(relay)
+                def _():
+                    for j in range(2):
+                        arrival(x_all.at[2 * origin + j], x_rs.at[l, 2 * origin + j], "tp").wait_recv()
+                        relay_copy(j).start()
+
             for k in reversed(range(dp)):
                 to = partner(me_d, k, dp)
                 for j in range(per):
                     t = to * per + j
 
-                    @pl.when(t != me_t)
+                    @pl.when((t != me_t) & jnp.logical_not(relay & (t // 2 == origin) & (quads > 3)))
                     def _():
                         arrival(x_all.at[t], x_rs.at[l, t], "tp").wait_recv()
 
@@ -255,11 +274,10 @@
         u_keep[l] = u
         pre = from_old[l] + jnp.dot(u, mix_w[l], precision=HIGHEST, preferred_element_type=F32) + skip_ref[l : l + 1, :] * u
         mix_all[l, me_d] = jax.nn.gelu(pre).astype(BF16)
-        for k in reversed(range(1, dp)):
+        for k in (*range(2, dp), 1) if l + 1 == layers else reversed(range(1, dp)):
             mix_copy(l, partner(me_d, k, dp)).start()
-        if l + 1 < layers:
-            for to in (*far, mate):
-                give_copy(l + 1, to).start()
+        if l + 1 == layers:
+            pl.when(held != home)(lambda: rest_copy().start())
         loads[l, 6].wait()
         loads[l, 7].wait()
 
@@ -279,7 +297,8 @@
                 def _():
                     comb_own[...] = total
 
-        for k in range(dp):
+        order = (0, 2, 1, *range(3, dp)) if l + 1 == layers else tuple(range(dp))
+        for n, k in enumerate(order):
             by = partner(me_d, k, dp, True)
             if k:
                 arrival(mix_all.at[l, by], mix_rs.at[l, by], "dp").wait_recv()
@@ -294,18 +313,18 @@
                 r = by * pairs + m
                 comb_send[l, 2 * r + 1 - side] = block[2 * r + 1 - side].astype(BF16)
                 pair_copy(l, r).start()
-            if k > 1:
-                pass_on(partner(me_d, k - 2, dp, True))
-        for k in range(max(dp - 2, 0), dp):
+            if n > 1:
+                pass_on(partner(me_d, order[n - 2], dp, True))
+        if l + 1 < layers:
+            for to in (*far, mate):
+                give_copy(l + 1, to).start()
+        for k in order[max(dp - 2, 0) :]:
             pass_on(partner(me_d, k, dp, True))
 
         if l + 1 == layers:
             update(l)
         if l + 1 < layers:
             prepare(l + 1)
-            for owner in far:
-                arrival(w_wide.at[l, owner], give_rs.at[l, owner], "dp").wait_recv()
-                pass_copy(l + 1, owner).start()
         combined = comb_own[...]
         for k in range(1, tp // 2):
             by = partner(me_p, k, tp // 2, True)
@@ -330,19 +349,29 @@
                 x_wide[l, me_d, me_t % per] = fresh
 
             if l + 2 == layers:
-                pl.when(held != home)(lambda: rest_copy().start())
 
                 @pl.when(held == home)
                 def _():
                     x_rest[...] = fresh
 
             update(l)
+            for owner in far:
+                arrival(w_wide.at[l, owner], give_rs.at[l, owner], "dp").wait_recv()
+                pass_copy(l + 1, owner).start()
         else:
             out_ref[...] = fresh
 
     for l in range(layers):
         for k in range(1, tp):
-            x_copy(l, k).wait_send()
+            gone = distant(partner(me_t, k, tp)) if l == 0 else False
+            pl.when(jnp.logical_not(gone))(lambda: x_copy(l, k).wait_send())
+        if l == 0 and quads > 3:
+
+            @pl.when(relay)
+            def _():
+                for j in range(2):
+                    relay_copy(j).wait_send()
+
         if l:
             pl.when(held != me_d)(lambda: x_copy(l, 0).wait_send())
             for to in (*far, mate):
@@ -437,7 +466,7 @@
             dma(layers, 8),
             dma(dp), dma(dp),
             dma(layers - 1, dp), dma(layers - 1, dp), dma(layers - 1, dp),
-            dma(1), dma(1),
+            dma(2), dma(1), dma(1),
             dma(layers, tp), dma(layers, tp),
             dma(dp), dma(dp),
             dma(dp), dma(dp),

time: 49.7 us -> 48.3 us (0.972)
  Pallas kernels: 49 us -> 47.5 us
    pallas_call x1, Pallas kernels: 48 us -> 46.5 us  [per_device(): pl.pallas_call(functools.partial(kernel, tp, dp, chans), out_shape=(pltpu...]
where the time goes in v3:
time: 48.3 us; the launch traced here: 48.1 us
  Pallas kernels  47.5 us (98%)
  between operations  0.64 us (1%)
    pallas_call x1, Pallas kernels, per_device(): pl.pallas_call(functools.partial(kernel, tp, dp, chans), out_shape=(pltpu...  46.5 us
    pallas_call x1, Pallas kernels, per_device(): pl.pallas_call(store, out_shape=(hbm_out(stream), jax.ShapeDtypeStruct((l...  1 us

profile of v3, /device:TPU:2, one launch (start us, length us, event | category | flops | bytes accessed | tf_op | source)
XLA Modules:
  0.0 48.1 jit_solution(14592306805547617952)
XLA Ops:
  0.6 46.5 %shard_map.149 = (bf16[32,512]{1,0:T(8,128)(2,1)S(1)}, f32[2,1024,128]{2,1,0:T(8,128)S(1)}) custom-call(bf16[32,512]{1,0:T(8,128)(2,1)} %stream_hbm.1, f32[2,512]{1,0:T(2,128)} %gain_hbm.1, bf16[2,512,256]{2,1,0:T(8,128)(2,1)} %w_in_hbm.1, f32[2,16,64]{2,1,0:T(8,128)} %lam_re_hbm.1, f32[2,16,64]{2,1,0:T(8,128)} %lam_im_hbm.1, f32[2,16]{1,0:T(2,128)} %log_dt_hbm.1, ...), custom_call_target="tpu_custom_call" | custom-call | tf_op jit(solution)/shard_map/pallas_call | solution.py:426
  47.1 1.0 %shard_map.150 = (bf16[32,512]{1,0:T(8,128)(2,1)}, f32[2,1024,128]{2,1,0:T(8,128)}) custom-call(bf16[32,512]{1,0:T(8,128)(2,1)S(1)} %get-tuple-element.6.x_ref, f32[2,1024,128]{2,1,0:T(8,128)S(1)} %get-tuple-element.7.state_ref), custom_call_target="tpu_custom_call" | custom-call | tf_op jit(solution)/shard_map/pallas_call | solution.py:484
